TPU v7x, 32 devices: a whole 2x2x4 slice. The times are simulated.
32 devices in a mesh: grp: 2 (over y), sp: 4 (over z), tp: 4 (over x, core).
Axes of the slice: x: 2, y: 2, z: 4, core: 2. Of those that a mesh axis runs over, the one named last changes fastest.
Arguments:
- carryover_vector: bfloat16 [2048, 2048], P(('grp', 'sp', 'tp')), parts along dimension 0, may hold values from -6 to 6
- channel_source_entries: bfloat16 [2048, 1024], P(('grp', 'sp'), 'tp'), parts along dimension 0, may hold values from -6 to 6
- final_modulation_vector: bfloat16 [2048, 1024], P(('grp', 'sp'), 'tp'), parts along dimension 0, may hold values from -54 to 54
- entering_basis_matrix: bfloat16 [2048, 512], P(('grp', 'sp'), 'tp'), parts along dimension 0, may hold values from -6 to 6
- readout_basis_matrix: bfloat16 [2048, 512], P(('grp', 'sp'), 'tp'), parts along dimension 0, may hold values from -6 to 6
- raw_stride_amount: float32 [2048, 16], P(('grp', 'sp'), 'tp'), parts along dimension 0, may hold values from -6 to 5
- extra_log_attenuation: float32 [2048, 16], P(('grp', 'sp'), 'tp'), parts along dimension 0, may hold values from -1.4 to 0
- channel_fading_rate: float32 [16], P('tp'), may hold values from 0 to 0.1, as said below
- channel_source_kernel: float32 [4, 1024], P(None, 'tp'), may hold values from -3 to 3
- entering_basis_kernel: float32 [4, 512], P(None, 'tp'), may hold values from -3 to 3
- readout_basis_kernel: float32 [4, 512], P(None, 'tp'), may hold values from -3 to 3
- modulated_rescaling_vector: float32 [1024], replicated, may hold values from 0.1 to 1.9
- blender_final_matrix: bfloat16 [1024, 2048], replicated, may hold values from -0.1875 to 0.1875
- specialist_rescaling_vector: float32 [2048], replicated, may hold values from 0.1 to 1.9
- specialist_gating_matrices: bfloat16 [8, 2048, 1024], P('sp', None, 'tp'), may hold values from -0.125 to 0.125
- widening_matrices: bfloat16 [8, 2048, 1024], P('sp', None, 'tp'), may hold values from -0.125 to 0.125
- contracting_matrices: bfloat16 [8, 1024, 2048], P('sp', 'tp'), may hold values from -0.1875 to 0.1875
- assigned_specialist_ids: int32 [2048, 2], P(('grp', 'sp')), parts along dimension 0, may hold values from 0 to 7, as said below
- specialist_choice_affinity: float32 [2048, 2], P(('grp', 'sp', 'tp')), parts along dimension 0, may hold values from -6 to 6
- cluster_chance: float32 [2048], P(('grp', 'sp', 'tp')), parts along dimension 0, may hold values from 0.25 to 1
Outputs:
- layer_out: bfloat16 [2048, 2048], P(('grp', 'sp', 'tp')), parts along dimension 0
There are 2 independent parts, one for each index of `grp`. A program takes and returns all parts, laid end to end along the dimension named above; an argument that names none is the same for every part. Nothing has to cross between parts.
Inputs may be any that keep to these rules, and one draw needn't show every extreme that they name: `assigned_specialist_ids`: each row names 2 different experts of one group: the experts g * 2 to (g + 1) * 2 - 1 for one g below 4. In each aligned block of 64 rows (the rows of one device) no expert is named by more than 32 rows, and every expert of one group, the same group in all blocks, is named by exactly 32 rows of every block. `channel_fading_rate`: positive.
All inputs are finite; a program needn't handle non-finite values.
Results may differ from a plain program's by a relative error of at most 0.015.
Values may be sent and summed in bfloat16 or wider, within the bound.
A program may use at most 64 MiB of HBM per device.

v0:
```python
import functools

import jax
import jax.numpy as jnp
from jax import lax
from jax.experimental import pallas as pl
from jax.experimental.pallas import tpu as pltpu
from jax.sharding import PartitionSpec as P

HEAD_DIM = 64
STATE = 128
EXPERT_GROUPS = 4
EPS = 1e-06
HIGHEST = lax.Precision.HIGHEST
F32 = jnp.float32
BF16 = jnp.bfloat16
TAIL = 16


def silu(v):
    return v / (1.0 + jnp.exp(-v))


def first_dims(a, b, precision=None):
    return lax.dot_general(
        a, b, (((0,), (0,)), ((), ())), precision=precision, preferred_element_type=F32
    )


def last_dims(a, b):
    return lax.dot_general(
        a, b, (((1,), (1,)), ((), ())), precision=HIGHEST, preferred_element_type=F32
    )


def spread(cols, width):
    heads = cols.shape[1]
    lane_head = lax.broadcasted_iota(jnp.int32, (cols.shape[0], width), 1) // HEAD_DIM
    out = jnp.broadcast_to(cols[:, 0:1], (cols.shape[0], width))
    for h in range(1, heads):
        out = jnp.where(lane_head == h, cols[:, h : h + 1], out)
    return out


def routing(meta, first_expert, rows, cap, locals_):
    id0, id1 = meta[0:1, :rows], meta[1:2, :rows]
    hit0 = (id0 >= first_expert) & (id0 < first_expert + locals_)
    hit1 = (id1 >= first_expert) & (id1 < first_expert + locals_)
    hit = jnp.where(hit0 | hit1, 1.0, 0.0)
    earlier = lax.broadcasted_iota(jnp.int32, (rows, rows), 0) < lax.broadcasted_iota(
        jnp.int32, (rows, rows), 1
    )
    place = jnp.dot(
        jnp.broadcast_to(hit, (8, rows)).astype(BF16),
        jnp.where(earlier, 1.0, 0.0).astype(BF16),
        preferred_element_type=F32,
    )[0:1]
    slot = lax.broadcasted_iota(jnp.int32, (cap, rows), 0).astype(F32)
    return jnp.where((place == slot) & (hit > 0.5), 1.0, 0.0)


def kernel(
    n,
    tp,
    cap,
    x_ref,
    b_ref,
    c_ref,
    z_ref,
    raw_ref,
    extra_ref,
    fade_ref,
    kx_ref,
    kb_ref,
    kc_ref,
    gain_ref,
    blend_hbm,
    sgain_ref,
    wg_hbm,
    wu_hbm,
    wd_hbm,
    ids_ref,
    aff_ref,
    chance_ref,
    carry_ref,
    out_ref,
    blend,
    wg,
    wu,
    wd,
    tail_x,
    tail_b,
    tail_c,
    ext,
    st_send,
    tot_send,
    st_buf,
    tot_buf,
    g_send,
    g_buf,
    mid,
    meta_ref,
    metas,
    x_send,
    arr,
    part,
    rs1,
    far_send,
    rs2,
    ret_send,
    ret,
    local_sem,
    tail_ss,
    tail_rs,
    st_ss,
    st_rs,
    tot_ss,
    tot_rs,
    meta_ss,
    meta_rs,
    g_ss,
    g_rs,
    z_ss,
    z_rs,
    far_ss,
    far_rs,
    near_ss,
    near_rs,
    p1_ss,
    p1_rs,
    p2_ss,
    p2_rs,
    ret_ss,
    ret_rs,
):
    s = lax.axis_index("sp")
    t = lax.axis_index("tp")
    length, width = x_ref.shape
    rows, model = carry_ref.shape
    heads = width // HEAD_DIM
    locals_ = wg_hbm.shape[0]
    far = (t + tp // 2) % tp
    near = t + 1 - 2 * (t % 2)
    near_far = (near + tp // 2) % tp

    def remote(src, dst, ssem, rsem, sp, tpi):
        return pltpu.make_async_remote_copy(
            src_ref=src,
            dst_ref=dst,
            send_sem=ssem,
            recv_sem=rsem,
            device_id={"sp": sp, "tp": tpi},
            device_id_type=pl.DeviceIdType.MESH,
        )

    barrier = pltpu.get_barrier_semaphore()
    for k in range(n):
        for q in range(tp):
            if k or q:
                pl.semaphore_signal(
                    barrier,
                    inc=1,
                    device_id={"sp": (s + k) % n, "tp": (t + q) % tp},
                    device_id_type=pl.DeviceIdType.MESH,
                )
    fetches = [
        pltpu.make_async_copy(src, dst, local_sem.at[i])
        for i, (src, dst) in enumerate(
            ((blend_hbm, blend), (wg_hbm, wg), (wu_hbm, wu), (wd_hbm, wd))
        )
    ]
    for fetch in fetches:
        fetch.start()

    dt_t = jnp.log1p(jnp.exp(raw_ref[...]))
    la_t = extra_ref[...] - fade_ref[...] * dt_t
    row_i = lax.broadcasted_iota(jnp.int32, (length, length), 0)
    col_i = lax.broadcasted_iota(jnp.int32, (length, length), 1)
    lower = row_i >= col_i
    cum = last_dims(jnp.where(lower, 1.0, 0.0), la_t)
    dt = last_dims(jnp.where(row_i == col_i, 1.0, 0.0), dt_t)
    cum_t = jnp.dot(
        la_t,
        jnp.where(row_i <= col_i, 1.0, 0.0),
        precision=HIGHEST,
        preferred_element_type=F32,
    )
    meta_ref[...] = jnp.zeros_like(meta_ref)
    ids = ids_ref[:, 0:rows]
    for i in range(1, tp):
        ids = jnp.where(t == i, ids_ref[:, i * rows : (i + 1) * rows], ids)
    meta_ref[0:2, 0:rows] = ids.astype(F32)
    meta_ref[2:4, 0:rows] = aff_ref[...]
    meta_ref[4:5, 0:rows] = chance_ref[...]

    pl.semaphore_wait(barrier, n * tp - 1)

    sends = []
    following = (s + 1) % n
    tails = []
    for i, (src, dst) in enumerate(((x_ref, tail_x), (b_ref, tail_b), (c_ref, tail_c))):
        copy = remote(
            src.at[pl.ds(length - TAIL, TAIL)], dst, tail_ss.at[i], tail_rs.at[i], following, t
        )
        copy.start()
        tails.append(copy)
    meta_copies = []
    for k in range(n):
        for q in range(tp):
            if k or q:
                copy = remote(
                    meta_ref,
                    metas.at[k, q],
                    meta_ss.at[k, q],
                    meta_rs.at[k, q],
                    (s + k) % n,
                    (t + q) % tp,
                )
                copy.start()
                meta_copies.append(copy)
    metas[0, 0] = meta_ref[...]

    ext[TAIL:, 0:width] = x_ref[...].astype(F32)
    ext[TAIL:, width : width + STATE] = b_ref[...].astype(F32)
    ext[TAIL:, width + STATE : width + 2 * STATE] = c_ref[...].astype(F32)
    for copy in tails:
        copy.wait()
    inner = s > 0
    ext[0:TAIL, 0:width] = jnp.where(inner, tail_x[...].astype(F32), 0.0)
    ext[0:TAIL, width : width + STATE] = jnp.where(inner, tail_b[...].astype(F32), 0.0)
    ext[0:TAIL, width + STATE : width + 2 * STATE] = jnp.where(
        inner, tail_c[...].astype(F32), 0.0
    )

    def conv(taps, first, count):
        kernel_len = taps.shape[0]
        total = None
        for j in range(kernel_len):
            at = TAIL - kernel_len + 1 + j
            term = taps[j : j + 1, :] * ext[at : at + length, first : first + count]
            total = term if total is None else total + term
        return silu(total)

    keys = conv(kb_ref, width, STATE).astype(BF16)
    xdt = conv(kx_ref, 0, width) * spread(dt, width)
    tot = cum[length - 1 : length, :]
    remain = jnp.exp(tot - cum)
    state = first_dims(keys, (xdt * spread(remain, width)).astype(BF16))
    st_send[...] = state.astype(BF16)
    tot_send[...] = jnp.broadcast_to(spread(tot, width), tot_send.shape)
    states = []
    for k in range(1, n):
        a = remote(st_send, st_buf.at[k], st_ss.at[k], st_rs.at[k], (s + k) % n, t)
        b = remote(tot_send, tot_buf.at[k], tot_ss.at[k], tot_rs.at[k], (s + k) % n, t)
        b.start()
        a.start()
        states += [a, b]

    queries = conv(kc_ref, width + STATE, STATE).astype(BF16)
    scores = lax.dot_general(
        queries, keys, (((1,), (1,)), ((), ())), preferred_element_type=F32
    )
    xdt_b = xdt.astype(BF16)
    lane_head = lax.broadcasted_iota(jnp.int32, (length, width), 1) // HEAD_DIM
    mixed = jnp.zeros((length, width), F32)
    for h in range(heads):
        between = jnp.where(lower, cum[:, h : h + 1] - cum_t[h : h + 1, :], -1e30)
        weights = (scores * jnp.exp(between)).astype(BF16)
        chosen = jnp.where(lane_head == h, xdt_b, jnp.zeros_like(xdt_b))
        mixed = mixed + jnp.dot(weights, chosen, preferred_element_type=F32)
    reach = jnp.exp(spread(cum, width))
    modulation = silu(z_ref[...].astype(F32))

    for copy in states:
        copy.wait()
    incoming = jnp.zeros((STATE, width), F32)
    for k in range(n - 1, 0, -1):
        later = incoming * jnp.exp(tot_buf[k, 0:1, :]) + st_buf[k].astype(F32)
        incoming = jnp.where(k <= s, later, incoming)
    outside = jnp.dot(queries, incoming.astype(BF16), preferred_element_type=F32)
    g_send[...] = ((mixed + outside * reach) * modulation).astype(BF16)
    spreads = []
    for q in (2, 3, 1) if tp == 4 else range(1, tp):
        to = (t + q) % tp
        copy = remote(
            g_send.at[pl.ds(to * rows, rows)], g_buf.at[t], g_ss.at[q], g_rs.at[q], s, to
        )
        copy.start()
        spreads.append(copy)
    g_buf[t] = g_send[pl.ds(pl.multiple_of(t * rows, rows), rows), :]

    own_meta = meta_ref[...]
    onehots = []
    for k in range(n):
        first = ((s + k) % n * locals_).astype(F32)
        onehots.append(routing(own_meta, first, rows, cap, locals_).astype(BF16))
    for copy in meta_copies:
        copy.wait()
    fetches[0].wait()
    for copy in spreads:
        copy.wait()
    squares = jnp.zeros((rows, 1), F32)
    for i in range(tp):
        piece = g_buf[i].astype(F32)
        squares = squares + jnp.sum(piece * piece, axis=1, keepdims=True)
    scale = lax.rsqrt(squares / (tp * width) + EPS)
    projected = carry_ref[...].astype(F32)
    for i in range(tp):
        span = slice(i * width, (i + 1) * width)
        normed = (g_buf[i].astype(F32) * scale * gain_ref[:, span]).astype(BF16)
        projected = projected + jnp.dot(normed, blend[span, :], preferred_element_type=F32)
    middle = projected.astype(BF16)
    mid[...] = middle
    wide = middle.astype(F32)
    expert_in = (
        wide
        * lax.rsqrt(jnp.mean(wide * wide, axis=1, keepdims=True) + EPS)
        * sgain_ref[...]
    ).astype(BF16)

    order = []
    for k in range(n // 2 + 1):
        for other in (k, (n - k) % n):
            if other not in order:
                order.append(other)

    z_copies, far_copies, near_copies, p1_copies, p2_copies, ret_copies = {}, {}, {}, {}, {}, {}
    for k in order[1:] + order[:1]:
        picked = jnp.dot(onehots[k], expert_in, preferred_element_type=F32).astype(BF16)
        if k == 0:
            arr[0, t] = picked
        else:
            x_send[k] = picked
            z_copies[k] = remote(
                x_send.at[k], arr.at[k, t], z_ss.at[k], z_rs.at[k], (s + k) % n, t
            )
            z_copies[k].start()

    def pass_far(k):
        if k:
            z_copies[k].wait()
        far_copies[k] = remote(arr.at[k, t], arr.at[k, t], far_ss.at[k], far_rs.at[k], s, far)
        far_copies[k].start()
        first = remote(
            arr.at[k, t], arr.at[k, t], near_ss.at[k, 0], near_rs.at[k, 0], s, near
        )
        first.start()
        near_copies[k] = [first]

    def pass_near(k):
        far_copies[k].wait()
        second = remote(
            arr.at[k, far], arr.at[k, far], near_ss.at[k, 1], near_rs.at[k, 1], s, near
        )
        second.start()
        near_copies[k].append(second)

    weight_row0 = s * locals_

    def slot_weights(k):
        columns = [[] for _ in range(locals_)]
        for i in range(tp):
            q = (t + tp - i) % tp
            meta = metas[k, q]
            onehot = routing(meta, weight_row0.astype(F32), rows, cap, locals_)
            for l in range(locals_):
                expert = (weight_row0 + l).astype(F32)
                lift0, lift1 = jnp.exp(meta[2:3, :rows]), jnp.exp(meta[3:4, :rows])
                share = meta[4:5, :rows] / (lift0 + lift1)
                mine = share * (
                    jnp.where(meta[0:1, :rows] == expert, lift0, 0.0)
                    + jnp.where(meta[1:2, :rows] == expert, lift1, 0.0)
                )
                columns[l].append(jnp.sum(onehot * mine, axis=1, keepdims=True))
        return [jnp.concatenate(c, axis=0) for c in columns]

    def experts(k):
        shares = slot_weights(k)
        for copy in near_copies[k]:
            copy.wait()
        tokens = arr[k].reshape(tp * cap, model)
        if not loaded:
            for fetch in fetches[1:]:
                fetch.wait()
            loaded.append(True)
        total = None
        for l in range(locals_):
            gate = jnp.dot(tokens, wg[l], preferred_element_type=F32)
            up = jnp.dot(tokens, wu[l], preferred_element_type=F32)
            hidden = (silu(gate) * up * shares[l]).astype(BF16)
            term = jnp.dot(hidden, wd[l], preferred_element_type=F32)
            total = term if total is None else total + term
        part[k] = total.astype(BF16).reshape(tp, cap, model)
        pair = []
        for i, owner in ((1, near_far), (0, near)):
            copy = remote(
                part.at[k, owner], rs1.at[k, i], p1_ss.at[k, i], p1_rs.at[k, i], s, near
            )
            copy.start()
            pair.append(copy)
        p1_copies[k] = pair

    def reduce_near(k):
        for copy in p1_copies[k]:
            copy.wait()
        far_send[k] = (part[k, far].astype(F32) + rs1[k, 1].astype(F32)).astype(BF16)
        p2_copies[k] = remote(far_send.at[k], rs2.at[k], p2_ss.at[k], p2_rs.at[k], s, far)
        p2_copies[k].start()

    def reduce_far(k):
        p2_copies[k].wait()
        total = (
            part[k, t].astype(F32) + rs1[k, 0].astype(F32) + rs2[k].astype(F32)
        ).astype(BF16)
        if k == 0:
            ret[0] = total
        else:
            ret_send[k] = total
            ret_copies[k] = remote(
                ret_send.at[k], ret.at[k], ret_ss.at[k], ret_rs.at[k], (s + n - k) % n, t
            )
            ret_copies[k].start()

    loaded = []
    pass_far(order[0])
    for i in range(n + 2):
        if i + 1 < n:
            pass_far(order[i + 1])
        if i < n:
            pass_near(order[i])
            experts(order[i])
        if 0 <= i - 1 < n:
            reduce_near(order[i - 1])
        if 0 <= i - 2 < n:
            reduce_far(order[i - 2])

    result = mid[...].astype(F32)
    for k in order:
        if k:
            ret_copies[k].wait()
        result = result + first_dims(onehots[k], ret[k])
    out_ref[...] = result.astype(BF16)


def per_device(
    n,
    tp,
    carryover_vector,
    channel_source_entries,
    final_modulation_vector,
    entering_basis_matrix,
    readout_basis_matrix,
    raw_stride_amount,
    extra_log_attenuation,
    channel_fading_rate,
    channel_source_kernel,
    entering_basis_kernel,
    readout_basis_kernel,
    modulated_rescaling_vector,
    blender_final_matrix,
    specialist_rescaling_vector,
    specialist_gating_matrices,
    widening_matrices,
    contracting_matrices,
    assigned_specialist_ids,
    specialist_choice_affinity,
    cluster_chance,
):
    length, width = channel_source_entries.shape
    rows, model = carryover_vector.shape
    locals_, _, hidden = specialist_gating_matrices.shape
    experts = n * locals_
    picks = assigned_specialist_ids.shape[1]
    assert tp == 4 and picks == 2 and entering_basis_matrix.shape[1] == STATE
    per_expert = 2 * rows * picks // experts
    group_size = experts // EXPERT_GROUPS
    if group_size <= locals_:
        cap = locals_ * per_expert // picks
    else:
        cap = locals_ * per_expert
    cap = -(-min(cap, rows) // 16) * 16
    vmem = pl.BlockSpec(memory_space=pltpu.VMEM)
    hbm = pl.BlockSpec(memory_space=pl.ANY)
    dma = pltpu.SemaphoreType.DMA
    scratch = [
        pltpu.VMEM(blender_final_matrix.shape, BF16),
        pltpu.VMEM(specialist_gating_matrices.shape, BF16),
        pltpu.VMEM(widening_matrices.shape, BF16),
        pltpu.VMEM(contracting_matrices.shape, BF16),
        pltpu.VMEM((TAIL, width), BF16),
        pltpu.VMEM((TAIL, STATE), BF16),
        pltpu.VMEM((TAIL, STATE), BF16),
        pltpu.VMEM((TAIL + length, width + 2 * STATE), F32),
        pltpu.VMEM((STATE, width), BF16),
        pltpu.VMEM((8, width), F32),
        pltpu.VMEM((n, STATE, width), BF16),
        pltpu.VMEM((n, 8, width), F32),
        pltpu.VMEM((length, width), BF16),
        pltpu.VMEM((tp, rows, width), BF16),
        pltpu.VMEM((rows, model), BF16),
        pltpu.VMEM((8, 128), F32),
        pltpu.VMEM((n, tp, 8, 128), F32),
        pltpu.VMEM((n, cap, model), BF16),
        pltpu.VMEM((n, tp, cap, model), BF16),
        pltpu.VMEM((n, tp, cap, model), BF16),
        pltpu.VMEM((n, 2, cap, model), BF16),
        pltpu.VMEM((n, cap, model), BF16),
        pltpu.VMEM((n, cap, model), BF16),
        pltpu.VMEM((n, cap, model), BF16),
        pltpu.VMEM((n, cap, model), BF16),
        dma((4,)),
    ]
    for shape in ((3,), (n,), (n,), (n, tp), (tp,), (n,), (n,), (n, 2), (n, 2), (n,), (n,)):
        scratch += [dma(shape), dma(shape)]
    return pl.pallas_call(
        functools.partial(kernel, n, tp, cap),
        out_shape=jax.ShapeDtypeStruct((rows, model), BF16),
        in_specs=[vmem] * 11 + [hbm, vmem, hbm, hbm, hbm] + [vmem] * 4,
        out_specs=vmem,
        scratch_shapes=scratch,
        compiler_params=pltpu.CompilerParams(
            collective_id=0, has_side_effects=True, vmem_limit_bytes=60 * 1024 * 1024
        ),
    )(
        channel_source_entries,
        entering_basis_matrix,
        readout_basis_matrix,
        final_modulation_vector,
        raw_stride_amount.T,
        extra_log_attenuation.T,
        channel_fading_rate[:, None],
        channel_source_kernel,
        entering_basis_kernel,
        readout_basis_kernel,
        modulated_rescaling_vector[None, :],
        blender_final_matrix,
        specialist_rescaling_vector[None, :],
        specialist_gating_matrices,
        widening_matrices,
        contracting_matrices,
        assigned_specialist_ids.T,
        specialist_choice_affinity.T,
        cluster_chance[None, :],
        carryover_vector,
    )


def solution(mesh):
    return jax.shard_map(
        functools.partial(per_device, mesh.shape["sp"], mesh.shape["tp"]),
        mesh=mesh,
        in_specs=(
            P(("grp", "sp", "tp"), None),
            P(("grp", "sp"), "tp"),
            P(("grp", "sp"), "tp"),
            P(("grp", "sp"), "tp"),
            P(("grp", "sp"), "tp"),
            P(("grp", "sp"), "tp"),
            P(("grp", "sp"), "tp"),
            P("tp"),
            P(None, "tp"),
            P(None, "tp"),
            P(None, "tp"),
            P(),
            P(),
            P(),
            P("sp", None, "tp"),
            P("sp", None, "tp"),
            P("sp", "tp", None),
            P(("grp", "sp"), None),
            P(("grp", "sp", "tp"), None),
            P(("grp", "sp", "tp")),
        ),
        out_specs=P(("grp", "sp", "tp"), None),
        check_vma=False,
    )
```

profile of v0, /device:TPU:0, one launch (start us, length us, event | category | flops | bytes accessed | tf_op | source)
XLA Modules:
  0.0 67.9 jit_solution(18017526770802614621)
XLA Ops:
  0.0 1.3 %copy.21.fade_ref = f32[4,1]{1,0:T(4,128)} copy(f32[4,1]{0,1:T(1,128)} %bitcast.15) | data formatting | bytes 32 | tf_op jit(solution)/shard_map/broadcast_in_dim | solution.py:531
  1.3 64.9 %shard_map.190 = bf16[64,2048]{1,0:T(8,128)(2,1)} custom-call(bf16[256,256]{1,0:T(8,128)(2,1)} %x_ref.1, bf16[256,128]{1,0:T(8,128)(2,1)} %b_ref.1, bf16[256,128]{1,0:T(8,128)(2,1)} %c_ref.1, bf16[256,256]{1,0:T(8,128)(2,1)} %z_ref.1, f32[4,256]{1,0:T(4,128)} %bitcast.9, f32[4,256]{1,0:T(4,128)} %bitcast.10, f32[4,1]{1,0:T(4,128)} %copy.21.fade_ref, ...), custom_call_target="tpu_custom_call" | custom-call | tf_op jit(solution)/shard_map/pallas_call | solution.py:515
  66.2 1.7 %copy.23 = bf16[64,2048]{1,0:T(8,128)(2,1)} copy(bf16[64,2048]{1,0:T(8,128)(2,1)} %shard_map.190) | data formatting | bytes 524288
where the time goes:
time: 68 us; the launch traced here: 67.9 us
  Pallas kernels  64.9 us (95%)
  local copies, waits for them, and re-layouts  2.98 us (4%)
    pallas_call x1, Pallas kernels, per_device(): pl.pallas_call(functools.partial(kernel, n, tp, cap), out_shape=jax.Shape...  64.9 us
    unnamed x1, local copies, waits for them, and re-layouts  1.67 us

commit v1 on v0

v1 whole, which is shorter than its diff:
```python
import functools

import jax
import jax.numpy as jnp
from jax import lax
from jax.experimental import pallas as pl
from jax.experimental.pallas import tpu as pltpu
from jax.sharding import PartitionSpec as P

HEAD_DIM = 64
STATE = 128
EXPERT_GROUPS = 4
EPS = 1e-06
HIGHEST = lax.Precision.HIGHEST
F32 = jnp.float32
BF16 = jnp.bfloat16
TAIL = 16
EXTRA = 128


def silu(v):
    return v / (1.0 + jnp.exp(-v))


def iota(shape, dim):
    return lax.broadcasted_iota(jnp.int32, shape, dim)


def first_dims(a, b, precision=None):
    return lax.dot_general(
        a, b, (((0,), (0,)), ((), ())), precision=precision, preferred_element_type=F32
    )


def last_dims(a, b):
    return lax.dot_general(
        a, b, (((1,), (1,)), ((), ())), precision=HIGHEST, preferred_element_type=F32
    )


def spread(cols, width):
    heads = cols.shape[1]
    lane_head = iota((cols.shape[0], width), 1) // HEAD_DIM
    out = jnp.broadcast_to(cols[:, 0:1], (cols.shape[0], width))
    for h in range(1, heads):
        out = jnp.where(lane_head == h, cols[:, h : h + 1], out)
    return out


def members(ids, n, locals_):
    count = -(-n // 8) * 8
    low = iota((count, ids.shape[1]), 0) * locals_
    id0, id1 = ids[0:1], ids[1:2]
    hit0 = (id0 >= low) & (id0 < low + locals_)
    hit1 = (id1 >= low) & (id1 < low + locals_)
    return jnp.where(hit0, 1.0, 0.0), jnp.where(hit0 | hit1, 1.0, 0.0)


def places(hit, rows):
    length = hit.shape[1]
    i, j = iota((length, length), 0), iota((length, length), 1)
    earlier = jnp.where((i < j) & (i // rows == j // rows), 1.0, 0.0).astype(BF16)
    return jnp.dot(hit.astype(BF16), earlier, preferred_element_type=F32)


def kernel(n, tp, cap, names, *refs):
    r = dict(zip(names, refs))
    s = lax.axis_index("sp")
    t = lax.axis_index("tp")
    length, width = r["x"].shape
    rows, model = r["carry"].shape
    heads = width // HEAD_DIM
    locals_ = r["wg"].shape[0]
    slots = tp * cap
    far = (t + tp // 2) % tp
    near = t + 1 - 2 * (t % 2)
    near_far = (near + tp // 2) % tp

    if n == 4:
        half = s // 2
        own = 0
        source = [
            s,
            half + (1 - half) * (1 - s),
            2 * (1 - half) + half * (5 - s),
            3 * (1 - half),
        ]
        routes = ([1, 2, 3], [2, 3, 0], [1, 0, 3], [2, 1, 0])
    else:
        own = s
        routes = [[d for d in range(n) if d != v] for v in range(n)]

    def source_of(j):
        return source[j] if n == 4 else j

    def early(v):
        return [("c", d) for d in (routes[v][:1] if v == 0 and n == 4 else routes[v])]

    def late(v):
        return [("g", d) for d in (routes[v][:1] if v == 0 and n == 4 else routes[v])]

    def last(v):
        return [("c", 3), ("g", 3), ("c", 2), ("g", 2)] if v == 0 and n == 4 else []

    def slot_at(d):
        if n != 4:
            return s
        if d < 2:
            return half * s + 1 - half
        return (1 - half) * (3 - 2 * s) + 2 * half

    def remote(src, dst, ssem, rsem, sp, tpi):
        return pltpu.make_async_remote_copy(
            src_ref=src,
            dst_ref=dst,
            send_sem=ssem,
            recv_sem=rsem,
            device_id={"sp": sp, "tp": tpi},
            device_id_type=pl.DeviceIdType.MESH,
        )

    barrier = pltpu.get_barrier_semaphore()
    peers = [((s + k) % n, t) for k in range(1, n)] + [(s, near), (s, far)]
    for sp, tpi in peers:
        pl.semaphore_signal(
            barrier,
            inc=1,
            device_id={"sp": sp, "tp": tpi},
            device_id_type=pl.DeviceIdType.MESH,
        )
    fetches = {}
    for i, name in enumerate(INPUTS):
        fetches[name] = pltpu.make_async_copy(r[name + "_hbm"], r[name], r["local_sem"].at[i])
        fetches[name].start()

    def fetched(*wanted):
        for name in wanted:
            fetches[name].wait()

    fetched("x", "b", "c")

    with jax.named_scope("barrier"):
        pl.semaphore_wait(barrier, len(peers))

    tails = []
    for i, name in enumerate("xbc"):
        copy = remote(
            r[name].at[pl.ds(length - TAIL, TAIL)],
            r["tail_" + name],
            r["tail_ss"].at[i],
            r["tail_rs"].at[i],
            (s + 1) % n,
            t,
        )
        copy.start()
        tails.append(copy)


    landing = {"c": r["carr"], "g": r["gbuf"]}

    def crossing(kind, d, place):
        return remote(
            r[kind + "_send"].at[d],
            landing[kind].at[place, t],
            r[kind + "z_ss"].at[d],
            r[kind + "z_rs"].at[place],
            d,
            t,
        )

    def dispatch(kind, d):
        crossing(kind, d, slot_at(d)).start()

    def dispatches(plan):
        for v in range(n):
            if plan(v):

                @pl.when(s == v)
                def _(v=v):
                    for kind, d in plan(v):
                        dispatch(kind, d)

    def across(kind, j):
        ref = landing[kind]
        return remote(
            ref.at[j, t], ref.at[j, t], r[kind + "f_ss"].at[j], r[kind + "f_rs"].at[j], s, far
        )

    def beside(kind, j, i):
        ref = landing[kind]
        block = far if i else t
        return remote(
            ref.at[j, block],
            ref.at[j, block],
            r[kind + "n_ss"].at[j, i],
            r[kind + "n_rs"].at[j, i],
            s,
            near,
        )

    def spread_out(kind, j):
        across(kind, j).start()
        beside(kind, j, 0).start()

    def pass_far(kind, j):
        with jax.named_scope(f"z_{kind}"):
            crossing(kind, (s + 1) % n, j).wait_recv()
        spread_out(kind, j)

    def pass_near(kind, j):
        with jax.named_scope(f"far_{kind}"):
            across(kind, j).wait()
        beside(kind, j, 1).start()

    def gathered(kind, j):
        with jax.named_scope(f"near_{kind}"):
            beside(kind, j, 0).wait()
            beside(kind, j, 1).wait()

    fetched("ids", "aff", "chance")
    ids_all = r["ids"][...]
    ids = ids_all[:, 0:rows]
    for i in range(1, tp):
        ids = jnp.where(t == i, ids_all[:, i * rows : (i + 1) * rows], ids)
    first, hit = members(ids, n, locals_)
    place = places(hit, rows)
    lift = jnp.exp(r["aff"][...])
    share = r["chance"][...] / (lift[0:1] + lift[1:2])
    slot = iota((cap, rows), 0).astype(F32)
    lane = iota((cap, EXTRA), 1)
    fetched("carry")
    carry = r["carry"][...]
    for d in range(n):
        onehot = jnp.where((place[d : d + 1] == slot) & (hit[d : d + 1] > 0.5), 1.0, 0.0)
        r["oh_own"][d] = onehot.astype(BF16)
        r["c_send"][d, :, 0:model] = jnp.dot(
            onehot.astype(BF16), carry, preferred_element_type=F32
        ).astype(BF16)
        flag = jnp.sum(onehot * first[d : d + 1], axis=1, keepdims=True)
        extra = jnp.where(lane == 2 * locals_, flag, 0.0)
        for l in range(locals_):
            expert = d * locals_ + l
            mine = share * (
                jnp.where(ids[0:1] == expert, lift[0:1], 0.0)
                + jnp.where(ids[1:2] == expert, lift[1:2], 0.0)
            )
            col = jnp.sum(onehot * mine, axis=1, keepdims=True)
            high = col.astype(BF16).astype(F32)
            extra = jnp.where(lane == 2 * l, high, extra)
            extra = jnp.where(lane == 2 * l + 1, col - high, extra)
        r["c_send"][d, :, model : model + EXTRA] = extra.astype(BF16)
    r["carr"][own, t] = r["c_send"][s]

    dispatches(early)
    spread_out("c", own)

    fetched("raw", "extra", "fade")
    dt_t = jnp.log1p(jnp.exp(r["raw"][...]))
    fade = jnp.broadcast_to(r["fade"][...], (heads, heads))
    fade = jnp.where(iota((heads, heads), 0) == iota((heads, heads), 1), fade, 0.0)
    la_t = r["extra"][...] - jnp.sum(fade, axis=1, keepdims=True) * dt_t
    row_i = iota((length, length), 0)
    col_i = iota((length, length), 1)
    lower = row_i >= col_i
    cum = last_dims(jnp.where(lower, 1.0, 0.0), la_t)
    dt = last_dims(jnp.where(row_i == col_i, 1.0, 0.0), dt_t)
    cum_t = jnp.dot(
        la_t,
        jnp.where(row_i <= col_i, 1.0, 0.0),
        precision=HIGHEST,
        preferred_element_type=F32,
    )

    ext = r["ext"]
    ext[TAIL:, 0:width] = r["x"][...].astype(F32)
    ext[TAIL:, width : width + STATE] = r["b"][...].astype(F32)
    ext[TAIL:, width + STATE : width + 2 * STATE] = r["c"][...].astype(F32)
    fetched("kx", "kb", "kc")
    with jax.named_scope("tails"):
        for copy in tails:
            copy.wait()
    inside = s > 0
    ext[0:TAIL, 0:width] = jnp.where(inside, r["tail_x"][...].astype(F32), 0.0)
    ext[0:TAIL, width : width + STATE] = jnp.where(inside, r["tail_b"][...].astype(F32), 0.0)
    ext[0:TAIL, width + STATE : width + 2 * STATE] = jnp.where(
        inside, r["tail_c"][...].astype(F32), 0.0
    )

    def conv(taps, first, count):
        kernel_len = taps.shape[0]
        total = None
        for j in range(kernel_len):
            at = TAIL - kernel_len + 1 + j
            term = taps[j : j + 1, :] * ext[at : at + length, first : first + count]
            total = term if total is None else total + term
        return silu(total)

    keys = conv(r["kb"], width, STATE).astype(BF16)
    xdt = conv(r["kx"], 0, width) * spread(dt, width)
    tot = cum[length - 1 : length, :]
    remain = jnp.exp(tot - cum)
    state = first_dims(keys, (xdt * spread(remain, width)).astype(BF16))
    r["st_send"][...] = state.astype(BF16)
    r["tot_send"][...] = jnp.broadcast_to(spread(tot, width), r["tot_send"].shape)

    def total_copy(k):
        return remote(
            r["tot_send"],
            r["tot_buf"].at[k],
            r["tot_ss"].at[k],
            r["tot_rs"].at[k],
            (s + k) % n,
            t,
        )

    def state_copy(k):
        return remote(
            r["st_send"],
            r["st_buf"].at[k],
            r["st_ss"].at[k],
            r["st_rs"].at[k],
            (s + k) % n,
            t,
        )

    if n == 4:

        @pl.when(s == 2)
        def _():
            total_copy(1).start()

        @pl.when(s % 2 == 0)
        def _():
            state_copy(1).start()

    else:
        for k in range(1, n):

            @pl.when(s + k < n)
            def _(k=k):
                total_copy(k).start()
                state_copy(k).start()

    first, hit = members(ids_all, n, locals_)
    place = places(hit, rows)
    slot_row, slot_pos = iota((slots, length), 0), iota((slots, length), 1)
    same = slot_row // cap == slot_pos // rows
    slot = (slot_row % cap).astype(F32)
    for d in range(n):
        onehot = same & (place[d : d + 1] == slot) & (hit[d : d + 1] > 0.5)
        r["oh_seg"][d] = jnp.where(onehot, 1.0, 0.0).astype(BF16)
    queries = conv(r["kc"], width + STATE, STATE).astype(BF16)
    scores = lax.dot_general(
        queries, keys, (((1,), (1,)), ((), ())), preferred_element_type=F32
    )
    xdt_b = xdt.astype(BF16)
    lane_head = iota((length, width), 1) // HEAD_DIM
    mixed = jnp.zeros((length, width), F32)
    for h in range(heads):
        between = jnp.where(lower, cum[:, h : h + 1] - cum_t[h : h + 1, :], -1e30)
        weights = (scores * jnp.exp(between)).astype(BF16)
        chosen = jnp.where(lane_head == h, xdt_b, jnp.zeros_like(xdt_b))
        mixed = mixed + jnp.dot(weights, chosen, preferred_element_type=F32)
    reach = jnp.exp(spread(cum, width))
    fetched("z")
    modulation = silu(r["z"][...].astype(F32))

    if n == 4:

        @pl.when(s == 1)
        def _():
            pass_far("c", 1)

        @pl.when(s == 2)
        def _():
            pass_far("c", 1)
            pass_far("c", 2)

        @pl.when(s == 3)
        def _():
            pass_far("c", 2)
            pass_far("c", 1)

    incoming = r["incoming"]
    incoming[...] = jnp.zeros_like(incoming)
    if n == 4:

        @pl.when(s == 1)
        def _():
            with jax.named_scope("state"):
                state_copy(1).wait_recv()
            before = r["st_buf"][1].astype(F32)
            incoming[...] = before
            r["st_send"][...] = (before * jnp.exp(r["tot_send"][0:1, :]) + state).astype(BF16)
            state_copy(1).start()
            state_copy(2).start()

        @pl.when(s == 2)
        def _():
            with jax.named_scope("state"):
                state_copy(1).wait_recv()
            incoming[...] = r["st_buf"][1].astype(F32)

        @pl.when(s == 3)
        def _():
            with jax.named_scope("state"):
                total_copy(1).wait_recv()
                state_copy(1).wait_recv()
                state_copy(2).wait_recv()
            incoming[...] = r["st_buf"][2].astype(F32) * jnp.exp(
                r["tot_buf"][1, 0:1, :]
            ) + r["st_buf"][1].astype(F32)

    else:
        for k in range(n - 1, 0, -1):

            @pl.when(k <= s)
            def _(k=k):
                total_copy(k).wait_recv()
                state_copy(k).wait_recv()
                incoming[...] = incoming[...] * jnp.exp(r["tot_buf"][k, 0:1, :]) + r["st_buf"][
                    k
                ].astype(F32)

    outside = jnp.dot(queries, incoming[...].astype(BF16), preferred_element_type=F32)
    gated = ((mixed + outside * reach) * modulation).astype(BF16)
    for d in range(n):
        picked = jnp.dot(r["oh_seg"][d], gated, preferred_element_type=F32)
        r["g_send"][d] = picked.astype(BF16).reshape(slots, width)
    r["gbuf"][own, t] = r["g_send"][s]
    dispatches(late)
    spread_out("g", own)

    with jax.named_scope("weights"):
        fetched("gain", "sgain", "blend", "wg", "wu", "wd")

    def experts(j, between=None):
        gathered("c", j)
        gathered("g", j)
        squares = jnp.zeros((slots, 1), F32)
        for i in range(tp):
            piece = r["gbuf"][j, i].astype(F32)
            squares = squares + jnp.sum(piece * piece, axis=1, keepdims=True)
        scale = lax.rsqrt(squares / (tp * width) + EPS)
        rowsin = r["carr"][j].reshape(slots, model + EXTRA)
        projected = rowsin[:, 0:model].astype(F32)
        for i in range(tp):
            span = slice(i * width, (i + 1) * width)
            normed = (r["gbuf"][j, i].astype(F32) * scale * r["gain"][:, span]).astype(BF16)
            projected = projected + jnp.dot(
                normed, r["blend"][span, :], preferred_element_type=F32
            )
        middle = projected.astype(BF16)
        r["mid"][...] = middle.reshape(tp, cap, model)
        r["keep"][j] = r["mid"][t]
        wide = middle.astype(F32)
        tokens = (
            wide
            * lax.rsqrt(jnp.mean(wide * wide, axis=1, keepdims=True) + EPS)
            * r["sgain"][...]
        ).astype(BF16)
        lots = rowsin[:, model : model + EXTRA].astype(F32)
        total = None
        for l in range(locals_):
            part_share = lots[:, 2 * l : 2 * l + 1] + lots[:, 2 * l + 1 : 2 * l + 2]
            gate = jnp.dot(tokens, r["wg"][l], preferred_element_type=F32)
            up = jnp.dot(tokens, r["wu"][l], preferred_element_type=F32)
            hidden = (silu(gate) * up * part_share).astype(BF16)
            term = jnp.dot(hidden, r["wd"][l], preferred_element_type=F32)
            total = term if total is None else total + term
            if l == 0 and between is not None:
                between()
        r["part"][j] = total.astype(BF16).reshape(tp, cap, model)
        near_copy(j, 1).start()
        near_copy(j, 0).start()

    def near_copy(j, i):
        return remote(
            r["part"].at[j, near if i == 0 else near_far],
            r["rs1"].at[j, i],
            r["p1_ss"].at[j, i],
            r["p1_rs"].at[j, i],
            s,
            near,
        )

    def far_copy(j):
        return remote(
            r["far_send"].at[j], r["rs2"].at[j], r["p2_ss"].at[j], r["p2_rs"].at[j], s, far
        )

    def reduce_near(j):
        with jax.named_scope("p1"):
            near_copy(j, 1).wait()
            near_copy(j, 0).wait()
        r["far_send"][j] = (
            r["part"][j, far].astype(F32) + r["rs1"][j, 1].astype(F32)
        ).astype(BF16)
        far_copy(j).start()

    def returning(j, place):
        return remote(
            r["ret_send"].at[j],
            r["ret"].at[place],
            r["ret_ss"].at[j],
            r["ret_rs"].at[place],
            source_of(j),
            t,
        )

    def reduce_far(j):
        with jax.named_scope("p2"):
            far_copy(j).wait()
        flag = r["carr"][j, t][:, model : model + EXTRA].astype(F32)
        r["ret_send"][j] = (
            r["keep"][j].astype(F32) * flag[:, 2 * locals_ : 2 * locals_ + 1]
            + r["part"][j, t].astype(F32)
            + r["rs1"][j, 0].astype(F32)
            + r["rs2"][j].astype(F32)
        ).astype(BF16)

        @pl.when(source_of(j) == s)
        def _():
            r["ret"][s] = r["ret_send"][j]

        @pl.when(source_of(j) != s)
        def _():
            returning(j, s).start()

    if n == 4:

        @pl.when(s > 0)
        def _():
            pass_far("g", 1)

        pass_near("c", 0)
        pass_near("g", 0)

        @pl.when(s == 3)
        def _():
            pass_far("g", 2)

        @pl.when(s > 0)
        def _():
            pass_near("c", 1)
            pass_near("g", 1)

        @pl.when(s == 3)
        def _():
            pass_far("c", 3)
            pass_far("g", 3)

        experts(0)
        dispatches(last)

        @pl.when(s == 0)
        def _():
            pass_far("c", 1)
            pass_far("g", 1)
            pass_far("c", 2)
            pass_near("c", 1)
            pass_near("g", 1)

        @pl.when(s == 1)
        def _():
            pass_far("c", 2)

        @pl.when(s < 3)
        def _():
            pass_far("g", 2)
            pass_far("c", 3)

        @pl.when(s < 2)
        def _():
            pass_far("g", 3)

        experts(1, lambda: reduce_near(0))

        @pl.when(s == 2)
        def _():
            pass_far("g", 3)

        pass_near("c", 2)
        pass_near("g", 2)
        experts(2, lambda: reduce_near(1))

        pass_near("c", 3)
        pass_near("g", 3)
        reduce_near(2)
        reduce_far(0)
        experts(3, lambda: reduce_far(1))
        reduce_near(3)
        reduce_far(2)
        reduce_far(3)
    else:

        def one(j, carried):
            @pl.when(j != s)
            def _():
                pass_far("c", j)
                pass_far("g", j)

            pass_near("c", j)
            pass_near("g", j)
            experts(j)
            reduce_near(j)
            reduce_far(j)
            return carried

        lax.fori_loop(0, n, one, 0)

    result = jnp.zeros((rows, model), F32)
    for d in range(n):

        @pl.when(s != d)
        def _(d=d):
            with jax.named_scope(f"ret_{d}"):
                returning(0, d).wait_recv()

        result = result + first_dims(r["oh_own"][d], r["ret"][d])
    r["out"][...] = result.astype(BF16)

    for j in range(n):

        @pl.when(s != j)
        def _(j=j):
            crossing("c", j, 0).wait_send()
            crossing("g", j, 0).wait_send()

        @pl.when(source_of(j) != s)
        def _(j=j):
            returning(j, s).wait_send()

    if n == 4:

        @pl.when(s == 2)
        def _():
            total_copy(1).wait_send()

        @pl.when(s % 2 == 0)
        def _():
            state_copy(1).wait_send()

        @pl.when(s == 1)
        def _():
            state_copy(1).wait_send()
            state_copy(2).wait_send()

    else:
        for k in range(1, n):

            @pl.when(s + k < n)
            def _(k=k):
                total_copy(k).wait_send()
                state_copy(k).wait_send()


INPUTS = ("x", "b", "c", "ids", "aff", "chance", "carry", "raw", "extra", "fade")
INPUTS += ("kx", "kb", "kc", "z", "gain", "sgain", "blend", "wg", "wu", "wd")


def per_device(
    n,
    tp,
    carryover_vector,
    channel_source_entries,
    final_modulation_vector,
    entering_basis_matrix,
    readout_basis_matrix,
    raw_stride_amount,
    extra_log_attenuation,
    channel_fading_rate,
    channel_source_kernel,
    entering_basis_kernel,
    readout_basis_kernel,
    modulated_rescaling_vector,
    blender_final_matrix,
    specialist_rescaling_vector,
    specialist_gating_matrices,
    widening_matrices,
    contracting_matrices,
    assigned_specialist_ids,
    specialist_choice_affinity,
    cluster_chance,
):
    length, width = channel_source_entries.shape
    rows, model = carryover_vector.shape
    locals_ = specialist_gating_matrices.shape[0]
    experts = n * locals_
    picks = assigned_specialist_ids.shape[1]
    assert tp == 4 and picks == 2 and entering_basis_matrix.shape[1] == STATE
    per_expert = 2 * rows * picks // experts
    group_size = experts // EXPERT_GROUPS
    if group_size <= locals_:
        cap = locals_ * per_expert // picks
    else:
        cap = locals_ * per_expert
    cap = -(-min(cap, rows) // 16) * 16
    slots = tp * cap
    given = dict(
        ids=assigned_specialist_ids.T,
        aff=specialist_choice_affinity.T,
        chance=cluster_chance[None, :],
        carry=carryover_vector,
        raw=raw_stride_amount.T,
        extra=extra_log_attenuation.T,
        fade=channel_fading_rate[None, :],
        x=channel_source_entries,
        b=entering_basis_matrix,
        c=readout_basis_matrix,
        kx=channel_source_kernel,
        kb=entering_basis_kernel,
        kc=readout_basis_kernel,
        z=final_modulation_vector,
        gain=modulated_rescaling_vector[None, :],
        sgain=specialist_rescaling_vector[None, :],
        blend=blender_final_matrix,
        wg=specialist_gating_matrices,
        wu=widening_matrices,
        wd=contracting_matrices,
    )
    operands = [pltpu.with_memory_space_constraint(given[name], pltpu.HBM) for name in INPUTS]
    vmem = pltpu.VMEM
    dma = pltpu.SemaphoreType.DMA
    scratch = {name: vmem(given[name].shape, given[name].dtype) for name in INPUTS}
    scratch |= dict(
        tail_x=vmem((TAIL, width), BF16),
        tail_b=vmem((TAIL, STATE), BF16),
        tail_c=vmem((TAIL, STATE), BF16),
        ext=vmem((TAIL + length, width + 2 * STATE), F32),
        st_send=vmem((STATE, width), BF16),
        tot_send=vmem((8, width), F32),
        st_buf=vmem((n, STATE, width), BF16),
        tot_buf=vmem((n, 8, width), F32),
        incoming=vmem((STATE, width), F32),
        oh_own=vmem((n, cap, rows), BF16),
        oh_seg=vmem((n, slots, length), BF16),
        c_send=vmem((n, cap, model + EXTRA), BF16),
        carr=vmem((n, tp, cap, model + EXTRA), BF16),
        g_send=vmem((n, slots, width), BF16),
        gbuf=vmem((n, tp, slots, width), BF16),
        mid=vmem((tp, cap, model), BF16),
        keep=vmem((n, cap, model), BF16),
        part=vmem((n, tp, cap, model), BF16),
        rs1=vmem((n, 2, cap, model), BF16),
        far_send=vmem((n, cap, model), BF16),
        rs2=vmem((n, cap, model), BF16),
        ret_send=vmem((n, cap, model), BF16),
        ret=vmem((n, cap, model), BF16),
        local_sem=dma((len(INPUTS),)),
    )
    for name, shape in dict(
        tail=(3,),
        st=(n,),
        tot=(n,),
        cz=(n,),
        cf=(n,),
        cn=(n, 2),
        gz=(n,),
        gf=(n,),
        gn=(n, 2),
        p1=(n, 2),
        p2=(n,),
        ret=(n,),
    ).items():
        scratch[name + "_ss"] = dma(shape)
        scratch[name + "_rs"] = dma(shape)
    names = [name + "_hbm" for name in INPUTS] + ["out"] + list(scratch)
    return pl.pallas_call(
        functools.partial(kernel, n, tp, cap, names),
        out_shape=pltpu.VMEM((rows, model), BF16),
        in_specs=[pl.BlockSpec(memory_space=pltpu.HBM)] * len(operands),
        out_specs=pl.BlockSpec(memory_space=pltpu.VMEM),
        scratch_shapes=list(scratch.values()),
        compiler_params=pltpu.CompilerParams(
            collective_id=0,
            has_side_effects=True,
            vmem_limit_bytes=(40 if n <= 8 else 60) * 1024 * 1024,
        ),
    )(*operands)


def solution(mesh):
    return jax.shard_map(
        functools.partial(per_device, mesh.shape["sp"], mesh.shape["tp"]),
        mesh=mesh,
        in_specs=(
            P(("grp", "sp", "tp"), None),
            P(("grp", "sp"), "tp"),
            P(("grp", "sp"), "tp"),
            P(("grp", "sp"), "tp"),
            P(("grp", "sp"), "tp"),
            P(("grp", "sp"), "tp"),
            P(("grp", "sp"), "tp"),
            P("tp"),
            P(None, "tp"),
            P(None, "tp"),
            P(None, "tp"),
            P(),
            P(),
            P(),
            P("sp", None, "tp"),
            P("sp", None, "tp"),
            P("sp", "tp", None),
            P(("grp", "sp"), None),
            P(("grp", "sp", "tp"), None),
            P(("grp", "sp", "tp")),
        ),
        out_specs=P(("grp", "sp", "tp"), None),
        check_vma=False,
    )
```

time: 68 us -> 55.5 us (0.82)
  Pallas kernels: 64.9 us -> 54.6 us
  local copies, waits for them, and re-layouts: 2.98 us -> 0.71 us
    pallas_call x1, Pallas kernels: 64.9 us -> 54.6 us  [per_device(): pl.pallas_call(functools.partial(kernel, n, tp, cap, names), out_shape=pl...]
    broadcast_in_dim x1 -> x0, local copies, waits for them, and re-layouts: 1.31 us -> none  [per_device(): channel_fading_rate[:, None]]
    unnamed x1, local copies, waits for them, and re-layouts: 1.67 us -> 0.71 us
where the time goes in v1:
time: 55.5 us; the launch traced here: 55.3 us
  Pallas kernels  54.6 us (98%)
  local copies, waits for them, and re-layouts  0.71 us (1%)
    pallas_call x1, Pallas kernels, per_device(): pl.pallas_call(functools.partial(kernel, n, tp, cap, names), out_shape=pl...  54.6 us

profile of v1, /device:TPU:0, one launch (start us, length us, event | category | flops | bytes accessed | tf_op | source)
XLA Modules:
  0.0 55.3 jit_solution(2755681046182295553)
XLA Ops:
  0.0 54.6 %shard_map.190 = bf16[64,2048]{1,0:T(8,128)(2,1)S(1)} custom-call(bf16[256,256]{1,0:T(8,128)(2,1)} %refs_0_.1, bf16[256,128]{1,0:T(8,128)(2,1)} %refs_1_.1, bf16[256,128]{1,0:T(8,128)(2,1)} %refs_2_.1, s32[2,256]{1,0:T(2,128)} %bitcast.12, f32[2,64]{1,0:T(2,128)} %bitcast.13, f32[1,64]{1,0:T(1,128)} %bitcast.14, bf16[64,2048]{1,0:T(8,128)(2,1)} %refs_6_.1, ...), custom_call_target="tpu_custom_call" | custom-call | tf_op jit(solution)/shard_map/pallas_call | solution.py:769
  54.6 0.7 %copy.22 = bf16[64,2048]{1,0:T(8,128)(2,1)} copy(bf16[64,2048]{1,0:T(8,128)(2,1)S(1)} %shard_map.190) | data formatting | bytes 524288

commit v2 on v1

--- a/solution.py
+++ b/solution.py
@@ -63,6 +63,10 @@
     return jnp.dot(hit.astype(BF16), earlier, preferred_element_type=F32)
 
 
+def halves_of(cap):
+    return 2 if cap % 32 == 0 else 1
+
+
 def kernel(n, tp, cap, names, *refs):
     r = dict(zip(names, refs))
     s = lax.axis_index("sp")
@@ -72,20 +76,20 @@
     heads = width // HEAD_DIM
     locals_ = r["wg"].shape[0]
     slots = tp * cap
+    halves = halves_of(cap)
+    part_rows = cap // halves
     far = (t + tp // 2) % tp
     near = t + 1 - 2 * (t % 2)
     near_far = (near + tp // 2) % tp
 
+    place4 = (1 + 3 * (s % 2)) * (1 + 15 * (s // 2))
+
+    def listed(row):
+        return sum(v * 4**i for i, v in enumerate(row)) // place4 % 4
+
     if n == 4:
-        half = s // 2
         own = 0
-        source = [
-            s,
-            half + (1 - half) * (1 - s),
-            2 * (1 - half) + half * (5 - s),
-            3 * (1 - half),
-        ]
-        routes = ([1, 2, 3], [2, 3, 0], [1, 0, 3], [2, 1, 0])
+        source = [listed([ORDER[v][j] for v in range(n)]) for j in range(n)]
     else:
         own = s
         routes = [[d for d in range(n) if d != v] for v in range(n)]
@@ -93,21 +97,13 @@
     def source_of(j):
         return source[j] if n == 4 else j
 
-    def early(v):
-        return [("c", d) for d in (routes[v][:1] if v == 0 and n == 4 else routes[v])]
-
-    def late(v):
-        return [("g", d) for d in (routes[v][:1] if v == 0 and n == 4 else routes[v])]
-
-    def last(v):
-        return [("c", 3), ("g", 3), ("c", 2), ("g", 2)] if v == 0 and n == 4 else []
+    def planned(stage, v):
+        if n == 4:
+            return [("c" if code < G else "g", code % 10) for code in SENDS[v][stage]]
+        return [("cg"[stage // 2], d) for d in routes[v]] if stage % 2 == 0 else []
 
     def slot_at(d):
-        if n != 4:
-            return s
-        if d < 2:
-            return half * s + 1 - half
-        return (1 - half) * (3 - 2 * s) + 2 * half
+        return listed([ORDER[d].index(v) for v in range(n)]) if n == 4 else s
 
     def remote(src, dst, ssem, rsem, sp, tpi):
         return pltpu.make_async_remote_copy(
@@ -121,6 +117,8 @@
 
     barrier = pltpu.get_barrier_semaphore()
     peers = [((s + k) % n, t) for k in range(1, n)] + [(s, near), (s, far)]
+    if n == 4:
+        peers.append((s + 1 - 2 * (s % 2), near))
     for sp, tpi in peers:
         pl.semaphore_signal(
             barrier,
@@ -142,28 +140,26 @@
     with jax.named_scope("barrier"):
         pl.semaphore_wait(barrier, len(peers))
 
-    tails = []
-    for i, name in enumerate("xbc"):
-        copy = remote(
-            r[name].at[pl.ds(length - TAIL, TAIL)],
-            r["tail_" + name],
-            r["tail_ss"].at[i],
-            r["tail_rs"].at[i],
-            (s + 1) % n,
-            t,
-        )
-        copy.start()
-        tails.append(copy)
-
+    tail_lanes = dict(x=(0, width), b=(width, STATE), c=(width + STATE, STATE))
+    for name, (first, count) in tail_lanes.items():
+        r["tail_send"][:, first : first + count] = r[name][length - TAIL :, :]
+    tails = remote(
+        r["tail_send"], r["tail"], r["tail_ss"].at[0], r["tail_rs"].at[0], (s + 1) % n, t
+    )
+
+    @pl.when(s < n - 1)
+    def _():
+        tails.start()
 
     landing = {"c": r["carr"], "g": r["gbuf"]}
 
-    def crossing(kind, d, place):
+    def crossing(kind, d, place, lands=None):
+        lands = d if lands is None else lands
         return remote(
             r[kind + "_send"].at[d],
             landing[kind].at[place, t],
-            r[kind + "z_ss"].at[d],
-            r[kind + "z_rs"].at[place],
+            r[kind + "z_ss"].at[(d + n - 1 - s) % n],
+            r[kind + "z_rs"].at[place - 1 if n == 4 else (place + n - 1 - lands) % n],
             d,
             t,
         )
@@ -171,13 +167,13 @@
     def dispatch(kind, d):
         crossing(kind, d, slot_at(d)).start()
 
-    def dispatches(plan):
+    def dispatches(stage):
         for v in range(n):
-            if plan(v):
+            if planned(stage, v):
 
                 @pl.when(s == v)
                 def _(v=v):
-                    for kind, d in plan(v):
+                    for kind, d in planned(stage, v):
                         dispatch(kind, d)
 
     def across(kind, j):
@@ -204,7 +200,7 @@
 
     def pass_far(kind, j):
         with jax.named_scope(f"z_{kind}"):
-            crossing(kind, (s + 1) % n, j).wait_recv()
+            crossing(kind, (s + 1) % n, j, s).wait_recv()
         spread_out(kind, j)
 
     def pass_near(kind, j):
@@ -251,7 +247,7 @@
         r["c_send"][d, :, model : model + EXTRA] = extra.astype(BF16)
     r["carr"][own, t] = r["c_send"][s]
 
-    dispatches(early)
+    dispatches(0)
     spread_out("c", own)
 
     fetched("raw", "extra", "fade")
@@ -276,15 +272,13 @@
     ext[TAIL:, width : width + STATE] = r["b"][...].astype(F32)
     ext[TAIL:, width + STATE : width + 2 * STATE] = r["c"][...].astype(F32)
     fetched("kx", "kb", "kc")
-    with jax.named_scope("tails"):
-        for copy in tails:
-            copy.wait()
-    inside = s > 0
-    ext[0:TAIL, 0:width] = jnp.where(inside, r["tail_x"][...].astype(F32), 0.0)
-    ext[0:TAIL, width : width + STATE] = jnp.where(inside, r["tail_b"][...].astype(F32), 0.0)
-    ext[0:TAIL, width + STATE : width + 2 * STATE] = jnp.where(
-        inside, r["tail_c"][...].astype(F32), 0.0
-    )
+    ext[0:TAIL, :] = jnp.zeros((TAIL, width + 2 * STATE), F32)
+
+    @pl.when(s > 0)
+    def _():
+        with jax.named_scope("tails"):
+            tails.wait_recv()
+        ext[0:TAIL, :] = r["tail"][...].astype(F32)
 
     def conv(taps, first, count):
         kernel_len = taps.shape[0]
@@ -307,8 +301,8 @@
         return remote(
             r["tot_send"],
             r["tot_buf"].at[k],
-            r["tot_ss"].at[k],
-            r["tot_rs"].at[k],
+            r["tot_ss"].at[k - 1],
+            r["tot_rs"].at[k - 1],
             (s + k) % n,
             t,
         )
@@ -317,8 +311,8 @@
         return remote(
             r["st_send"],
             r["st_buf"].at[k],
-            r["st_ss"].at[k],
-            r["st_rs"].at[k],
+            r["st_ss"].at[k - 1],
+            r["st_rs"].at[k - 1],
             (s + k) % n,
             t,
         )
@@ -340,6 +334,8 @@
             def _(k=k):
                 total_copy(k).start()
                 state_copy(k).start()
+
+    dispatches(1)
 
     first, hit = members(ids_all, n, locals_)
     place = places(hit, rows)
@@ -365,22 +361,37 @@
     fetched("z")
     modulation = silu(r["z"][...].astype(F32))
 
-    if n == 4:
-
-        @pl.when(s == 1)
-        def _():
-            pass_far("c", 1)
-
-        @pl.when(s == 2)
-        def _():
-            pass_far("c", 1)
-            pass_far("c", 2)
-
-        @pl.when(s == 3)
-        def _():
-            pass_far("c", 2)
-            pass_far("c", 1)
-
+    def steps(at):
+        for v in range(n):
+            if n == 4 and STEPS[v].get(at):
+
+                @pl.when(s == v)
+                def _(v=v):
+                    for step in STEPS[v][at]:
+                        if step == LAST:
+                            pl.semaphore_wait(r["clear"], 2)
+                            for kind, d in planned(3, v):
+                                dispatch(kind, d)
+                        elif step == CLEAR:
+                            state_copy(1).wait_send()
+                            state_copy(2).wait_send()
+                            for tpi in (t, near):
+                                pl.semaphore_signal(
+                                    r["clear"],
+                                    inc=1,
+                                    device_id={"sp": s - 1, "tp": tpi},
+                                    device_id_type=pl.DeviceIdType.MESH,
+                                )
+                        else:
+                            acts[step - step % 10](step % 10)
+
+    acts = {
+        FC: functools.partial(pass_far, "c"),
+        FG: functools.partial(pass_far, "g"),
+        NC: functools.partial(pass_near, "c"),
+        NG: functools.partial(pass_near, "g"),
+    }
+    steps("pre")
     incoming = r["incoming"]
     incoming[...] = jnp.zeros_like(incoming)
     if n == 4:
@@ -428,7 +439,7 @@
         picked = jnp.dot(r["oh_seg"][d], gated, preferred_element_type=F32)
         r["g_send"][d] = picked.astype(BF16).reshape(slots, width)
     r["gbuf"][own, t] = r["g_send"][s]
-    dispatches(late)
+    dispatches(2)
     spread_out("g", own)
 
     with jax.named_scope("weights"):
@@ -484,114 +495,67 @@
             near,
         )
 
-    def far_copy(j):
+    def half_rows(h):
+        return pl.ds(h * part_rows, part_rows)
+
+    def far_copy(j, h):
         return remote(
-            r["far_send"].at[j], r["rs2"].at[j], r["p2_ss"].at[j], r["p2_rs"].at[j], s, far
+            r["far_send"].at[j, half_rows(h)],
+            r["rs2"].at[j, half_rows(h)],
+            r["p2_ss"].at[j, h],
+            r["p2_rs"].at[j, h],
+            s,
+            far,
         )
 
     def reduce_near(j):
         with jax.named_scope("p1"):
             near_copy(j, 1).wait()
             near_copy(j, 0).wait()
-        r["far_send"][j] = (
-            r["part"][j, far].astype(F32) + r["rs1"][j, 1].astype(F32)
-        ).astype(BF16)
-        far_copy(j).start()
-
-    def returning(j, place):
+        for h in range(halves):
+            at = half_rows(h)
+            r["far_send"][j, at] = (
+                r["part"][j, far, at].astype(F32) + r["rs1"][j, 1, at].astype(F32)
+            ).astype(BF16)
+            far_copy(j, h).start()
+
+    def returning(j, place, h, lands):
         return remote(
-            r["ret_send"].at[j],
-            r["ret"].at[place],
-            r["ret_ss"].at[j],
-            r["ret_rs"].at[place],
+            r["ret_send"].at[j, half_rows(h)],
+            r["ret"].at[place, half_rows(h)],
+            r["ret_ss"].at[max(j - 1, 0) if n == 4 else (source_of(j) + n - 1 - s) % n, h],
+            r["ret_rs"].at[(place + n - 1 - lands) % n, h],
             source_of(j),
             t,
         )
 
     def reduce_far(j):
-        with jax.named_scope("p2"):
-            far_copy(j).wait()
-        flag = r["carr"][j, t][:, model : model + EXTRA].astype(F32)
-        r["ret_send"][j] = (
-            r["keep"][j].astype(F32) * flag[:, 2 * locals_ : 2 * locals_ + 1]
-            + r["part"][j, t].astype(F32)
-            + r["rs1"][j, 0].astype(F32)
-            + r["rs2"][j].astype(F32)
-        ).astype(BF16)
+        lanes = slice(model + 2 * locals_, model + 2 * locals_ + 1)
+        for h in range(halves):
+            at = half_rows(h)
+            with jax.named_scope("p2"):
+                far_copy(j, h).wait()
+            r["ret_send"][j, at] = (
+                r["keep"][j, at].astype(F32) * r["carr"][j, t, at, lanes].astype(F32)
+                + r["part"][j, t, at].astype(F32)
+                + r["rs1"][j, 0, at].astype(F32)
+                + r["rs2"][j, at].astype(F32)
+            ).astype(BF16)
+
+            @pl.when(source_of(j) != s)
+            def _(h=h):
+                returning(j, s, h, source_of(j)).start()
 
         @pl.when(source_of(j) == s)
         def _():
             r["ret"][s] = r["ret_send"][j]
 
-        @pl.when(source_of(j) != s)
-        def _():
-            returning(j, s).start()
-
+    acts |= {RN: reduce_near, RF: reduce_far}
     if n == 4:
-
-        @pl.when(s > 0)
-        def _():
-            pass_far("g", 1)
-
-        pass_near("c", 0)
-        pass_near("g", 0)
-
-        @pl.when(s == 3)
-        def _():
-            pass_far("g", 2)
-
-        @pl.when(s > 0)
-        def _():
-            pass_near("c", 1)
-            pass_near("g", 1)
-
-        @pl.when(s == 3)
-        def _():
-            pass_far("c", 3)
-            pass_far("g", 3)
-
-        experts(0)
-        dispatches(last)
-
-        @pl.when(s == 0)
-        def _():
-            pass_far("c", 1)
-            pass_far("g", 1)
-            pass_far("c", 2)
-            pass_near("c", 1)
-            pass_near("g", 1)
-
-        @pl.when(s == 1)
-        def _():
-            pass_far("c", 2)
-
-        @pl.when(s < 3)
-        def _():
-            pass_far("g", 2)
-            pass_far("c", 3)
-
-        @pl.when(s < 2)
-        def _():
-            pass_far("g", 3)
-
-        experts(1, lambda: reduce_near(0))
-
-        @pl.when(s == 2)
-        def _():
-            pass_far("g", 3)
-
-        pass_near("c", 2)
-        pass_near("g", 2)
-        experts(2, lambda: reduce_near(1))
-
-        pass_near("c", 3)
-        pass_near("g", 3)
-        reduce_near(2)
-        reduce_far(0)
-        experts(3, lambda: reduce_far(1))
-        reduce_near(3)
-        reduce_far(2)
-        reduce_far(3)
+        steps("a")
+        for j in range(n):
+            experts(j, lambda: steps(f"m{j}"))
+            steps("bcde"[j])
     else:
 
         def one(j, carried):
@@ -615,21 +579,28 @@
         @pl.when(s != d)
         def _(d=d):
             with jax.named_scope(f"ret_{d}"):
-                returning(0, d).wait_recv()
+                for h in range(halves):
+                    returning(1, d, h, s).wait_recv()
 
         result = result + first_dims(r["oh_own"][d], r["ret"][d])
-    r["out"][...] = result.astype(BF16)
+    with jax.named_scope("store"):
+        r["out"][...] = result.astype(BF16)
+
+    @pl.when(s < n - 1)
+    def _():
+        tails.wait_send()
 
     for j in range(n):
 
         @pl.when(s != j)
         def _(j=j):
-            crossing("c", j, 0).wait_send()
-            crossing("g", j, 0).wait_send()
+            crossing("c", j, slot_at(j)).wait_send()
+            crossing("g", j, slot_at(j)).wait_send()
 
         @pl.when(source_of(j) != s)
         def _(j=j):
-            returning(j, s).wait_send()
+            for h in range(halves):
+                returning(j, s, h, source_of(j)).wait_send()
 
     if n == 4:
 
@@ -640,11 +611,6 @@
         @pl.when(s % 2 == 0)
         def _():
             state_copy(1).wait_send()
-
-        @pl.when(s == 1)
-        def _():
-            state_copy(1).wait_send()
-            state_copy(2).wait_send()
 
     else:
         for k in range(1, n):
@@ -657,6 +623,59 @@
 
 INPUTS = ("x", "b", "c", "ids", "aff", "chance", "carry", "raw", "extra", "fade")
 INPUTS += ("kx", "kb", "kc", "z", "gain", "sgain", "blend", "wg", "wu", "wd")
+
+
+FC, FG, NC, NG, RN, RF, LAST, CLEAR = range(10, 90, 10)
+C, G = 0, 10
+ORDER = ((0, 1, 2, 3), (1, 0, 2, 3), (2, 0, 1, 3), (3, 2, 0, 1))
+SENDS = (
+    ((), (C + 2, C + 1,), (G + 1,), (G + 2, C + 3, G + 3,)),
+    ((C + 2, C + 0,), (), (G + 2, C + 3, G + 3, G + 0,), ()),
+    ((C + 1, C + 0, C + 3,), (), (G + 1, G + 0, G + 3,), ()),
+    ((C + 2, C + 1, C + 0,), (), (G + 2, G + 1, G + 0,), ()),
+)
+STEPS = (
+    dict(
+        a=(FC + 1, NC + 0, NG + 0,),
+        b=(LAST, FC + 3, NC + 1, FG + 1, FC + 2, NG + 1, FG + 2,),
+        m1=(FG + 3,),
+        c=(NC + 2, NC + 3, NG + 2, RN + 1,),
+        m2=(NG + 3,),
+        m3=(RN + 2,),
+        e=(RF + 1, RN + 3, RF + 2, RN + 0, RF + 3, RF + 0,),
+    ),
+    dict(
+        a=(CLEAR, NC + 0, FC + 3, NG + 0, FC + 2,),
+        m0=(FC + 1,),
+        b=(FG + 1, NC + 2, FG + 2, NC + 1, FG + 3, NG + 1,),
+        m1=(NG + 2,),
+        c=(NC + 3,),
+        m2=(RN + 1, NG + 3,),
+        m3=(RN + 2,),
+        e=(RN + 3, RF + 1, RF + 2, RN + 0, RF + 3, RF + 0,),
+    ),
+    dict(
+        pre=(FC + 2, FC + 3,),
+        a=(FC + 1, NC + 2, NC + 3, NC + 0, FG + 1, NG + 0,),
+        m0=(FG + 3,),
+        b=(NC + 1, FG + 2, NG + 1,),
+        m1=(RN + 0,),
+        c=(NG + 2,),
+        m2=(RN + 1, NG + 3,),
+        m3=(RN + 2,),
+        e=(RF + 1, RN + 3, RF + 2, RF + 3, RF + 0,),
+    ),
+    dict(
+        pre=(FC + 1,),
+        a=(NC + 1, NC + 0, FG + 1, NG + 0,),
+        m0=(NG + 1, FC + 2,),
+        b=(FG + 2,),
+        c=(FC + 3, FG + 3, NC + 2, NG + 2,),
+        m2=(RN + 1,),
+        d=(NC + 3, NG + 3, RN + 2,),
+        e=(RF + 1, RN + 3, RF + 2, RN + 0, RF + 3, RF + 0,),
+    ),
+)
 
 
 def per_device(
@@ -723,10 +742,10 @@
     vmem = pltpu.VMEM
     dma = pltpu.SemaphoreType.DMA
     scratch = {name: vmem(given[name].shape, given[name].dtype) for name in INPUTS}
+    reach = 2 if n == 4 else n - 1
     scratch |= dict(
-        tail_x=vmem((TAIL, width), BF16),
-        tail_b=vmem((TAIL, STATE), BF16),
-        tail_c=vmem((TAIL, STATE), BF16),
+        tail_send=vmem((TAIL, width + 2 * STATE), BF16),
+        tail=vmem((TAIL, width + 2 * STATE), BF16),
         ext=vmem((TAIL + length, width + 2 * STATE), F32),
         st_send=vmem((STATE, width), BF16),
         tot_send=vmem((8, width), F32),
@@ -748,20 +767,21 @@
         ret_send=vmem((n, cap, model), BF16),
         ret=vmem((n, cap, model), BF16),
         local_sem=dma((len(INPUTS),)),
+        clear=pltpu.SemaphoreType.REGULAR,
     )
     for name, shape in dict(
-        tail=(3,),
-        st=(n,),
-        tot=(n,),
-        cz=(n,),
+        tail=(1,),
+        st=(reach,),
+        tot=(1 if n == 4 else reach,),
+        cz=(n - 1,),
         cf=(n,),
         cn=(n, 2),
-        gz=(n,),
+        gz=(n - 1,),
         gf=(n,),
         gn=(n, 2),
         p1=(n, 2),
-        p2=(n,),
-        ret=(n,),
+        p2=(n, halves_of(cap)),
+        ret=(n - 1, halves_of(cap)),
     ).items():
         scratch[name + "_ss"] = dma(shape)
         scratch[name + "_rs"] = dma(shape)

time: 55.5 us -> 51.1 us (0.921)
  the two profiles are of different devices: /device:TPU:0 before, /device:TPU:28 now
where the time goes in v2:
time: 51.1 us; the launch traced here: 50.9 us
  Pallas kernels  50.2 us (98%)
  local copies, waits for them, and re-layouts  0.71 us (1%)
    pallas_call x1, Pallas kernels, per_device(): pl.pallas_call(functools.partial(kernel, n, tp, cap, names), out_shape=pl...  50.2 us

profile of v2, /device:TPU:28, one launch (start us, length us, event | category | flops | bytes accessed | tf_op | source)
XLA Modules:
  0.0 50.9 jit_solution(15793708600654611421)
XLA Ops:
  0.0 50.2 %shard_map.190 = bf16[64,2048]{1,0:T(8,128)(2,1)S(1)} custom-call(bf16[256,256]{1,0:T(8,128)(2,1)} %refs_0_.1, bf16[256,128]{1,0:T(8,128)(2,1)} %refs_1_.1, bf16[256,128]{1,0:T(8,128)(2,1)} %refs_2_.1, s32[2,256]{1,0:T(2,128)} %bitcast.12, f32[2,64]{1,0:T(2,128)} %bitcast.13, f32[1,64]{1,0:T(1,128)} %bitcast.14, bf16[64,2048]{1,0:T(8,128)(2,1)} %refs_6_.1, ...), custom_call_target="tpu_custom_call" | custom-call | tf_op jit(solution)/shard_map/pallas_call | solution.py:789
  50.2 0.7 %copy.22 = bf16[64,2048]{1,0:T(8,128)(2,1)} copy(bf16[64,2048]{1,0:T(8,128)(2,1)S(1)} %shard_map.190) | data formatting | bytes 524288

commit v3 on v2

--- a/solution.py
+++ b/solution.py
@@ -631,16 +631,16 @@
 SENDS = (
     ((), (C + 2, C + 1,), (G + 1,), (G + 2, C + 3, G + 3,)),
     ((C + 2, C + 0,), (), (G + 2, C + 3, G + 3, G + 0,), ()),
-    ((C + 1, C + 0, C + 3,), (), (G + 1, G + 0, G + 3,), ()),
+    ((C + 1, C + 0, C + 3,), (), (G + 0, G + 1, G + 3,), ()),
     ((C + 2, C + 1, C + 0,), (), (G + 2, G + 1, G + 0,), ()),
 )
 STEPS = (
     dict(
         a=(FC + 1, NC + 0, NG + 0,),
-        b=(LAST, FC + 3, NC + 1, FG + 1, FC + 2, NG + 1, FG + 2,),
-        m1=(FG + 3,),
-        c=(NC + 2, NC + 3, NG + 2, RN + 1,),
-        m2=(NG + 3,),
+        b=(LAST, FC + 3, NC + 1, FG + 1, FC + 2, FG + 2, NG + 1,),
+        m1=(FG + 3, NC + 2,),
+        c=(NC + 3, NG + 2,),
+        m2=(RN + 1, NG + 3,),
         m3=(RN + 2,),
         e=(RF + 1, RN + 3, RF + 2, RN + 0, RF + 3, RF + 0,),
     ),

time: 51.1 us -> 50.6 us (level)
  the two profiles are of different devices: /device:TPU:28 before, /device:TPU:24 now
where the time goes in v3:
time: 50.6 us; the launch traced here: 50.5 us
  Pallas kernels  49.8 us (98%)
  local copies, waits for them, and re-layouts  0.71 us (1%)
    pallas_call x1, Pallas kernels, per_device(): pl.pallas_call(functools.partial(kernel, n, tp, cap, names), out_shape=pl...  49.8 us

profile of v3, /device:TPU:24, one launch (start us, length us, event | category | flops | bytes accessed | tf_op | source)
XLA Modules:
  0.0 50.5 jit_solution(1394732030374659216)
XLA Ops:
  0.0 49.8 %shard_map.190 = bf16[64,2048]{1,0:T(8,128)(2,1)S(1)} custom-call(bf16[256,256]{1,0:T(8,128)(2,1)} %refs_0_.1, bf16[256,128]{1,0:T(8,128)(2,1)} %refs_1_.1, bf16[256,128]{1,0:T(8,128)(2,1)} %refs_2_.1, s32[2,256]{1,0:T(2,128)} %bitcast.12, f32[2,64]{1,0:T(2,128)} %bitcast.13, f32[1,64]{1,0:T(1,128)} %bitcast.14, bf16[64,2048]{1,0:T(8,128)(2,1)} %refs_6_.1, ...), custom_call_target="tpu_custom_call" | custom-call | tf_op jit(solution)/shard_map/pallas_call | solution.py:789
  49.8 0.7 %copy.22 = bf16[64,2048]{1,0:T(8,128)(2,1)} copy(bf16[64,2048]{1,0:T(8,128)(2,1)S(1)} %shard_map.190) | data formatting | bytes 524288
